TPU v7x, 32 devices: a whole 2x2x4 slice. The times are simulated.
32 devices in a mesh: grp: 2 (over x), fs: 4 (over y, core), tp: 4 (over z).
Axes of the slice: x: 2, y: 2, z: 4, core: 2. Of those that a mesh axis runs over, the one named last changes fastest.
Arguments:
- stream: bfloat16 [4096, 2048], P(('grp', 'fs', 'tp')), parts along dimension 0, may hold values from -4 to 4
- gain_first: bfloat16 [2048], replicated, may hold values from 0.099609375 to 1.8984375
- gate_first: bfloat16 [2048, 4096], P('fs', 'tp'), may hold values from -0.125 to 0.125
- up_first: bfloat16 [2048, 4096], P('fs', 'tp'), may hold values from -0.125 to 0.125
- down_first: bfloat16 [4096, 2048], P('tp', 'fs'), may hold values from -0.09375 to 0.09375
- gain_second: bfloat16 [2048], replicated, may hold values from 0.099609375 to 1.8984375
- gate_second: bfloat16 [2048, 4096], P('fs', 'tp'), may hold values from -0.125 to 0.125
- up_second: bfloat16 [2048, 4096], P('fs', 'tp'), may hold values from -0.125 to 0.125
- down_second: bfloat16 [4096, 2048], P('tp', 'fs'), may hold values from -0.09375 to 0.09375
Outputs:
- result: bfloat16 [4096, 2048], P(('grp', 'fs', 'tp')), parts along dimension 0
There are 2 independent parts, one for each index of `grp`. A program takes and returns all parts, laid end to end along the dimension named above; an argument that names none is the same for every part. Nothing has to cross between parts.
All inputs are finite; a program needn't handle non-finite values.
Results may differ from a plain program's by a relative error of at most 0.018.
Values may be sent and summed in bfloat16 or wider, within the bound.
No kernel may reach another device: no remote copies, remote signals or barrier semaphores. Data moves between devices by JAX's collectives and lax.ppermute only.
A program may use at most 64 MiB of HBM per device.

v0:
```python
import jax
import jax.numpy as jnp
from jax import lax
from jax.sharding import PartitionSpec as P


def half_branch(stream, gain, gathered):
    stream_f = stream.astype(jnp.float32)
    normed = (
        stream_f
        * lax.rsqrt(jnp.mean(stream_f * stream_f, axis=-1, keepdims=True) + 1e-06)
        * gain.astype(jnp.float32)
    ).astype(jnp.bfloat16)
    tokens = lax.all_gather(normed, "tp", axis=0, tiled=True)
    gate_act = jnp.dot(tokens, gathered[0], preferred_element_type=jnp.float32)
    up_act = jnp.dot(tokens, gathered[1], preferred_element_type=jnp.float32)
    down_full = gathered[2]
    hidden = (jax.nn.silu(gate_act) * up_act).astype(jnp.bfloat16)
    summed = lax.psum_scatter(
        jnp.dot(hidden, down_full, preferred_element_type=jnp.float32).astype(jnp.bfloat16),
        "tp",
        scatter_dimension=0,
        tiled=True,
    ).astype(jnp.float32)
    return (stream_f + 0.5 * summed).astype(jnp.bfloat16)


def local(
    stream,
    gain_first,
    gate_first,
    up_first,
    down_first,
    gain_second,
    gate_second,
    up_second,
    down_second,
):
    weights = (
        lax.all_gather(gate_first, "fs", axis=0, tiled=True),
        lax.all_gather(up_first, "fs", axis=0, tiled=True),
        lax.all_gather(down_first, "fs", axis=1, tiled=True),
        lax.all_gather(gate_second, "fs", axis=0, tiled=True),
        lax.all_gather(up_second, "fs", axis=0, tiled=True),
        lax.all_gather(down_second, "fs", axis=1, tiled=True),
    )
    first_set = (weights[0], weights[1], weights[2])
    second_set = (weights[3], weights[4], weights[5])
    middle = half_branch(stream, gain_first, first_set)
    return half_branch(middle, gain_second, second_set)


def solution(mesh):
    in_specs = (
        P(("grp", "fs", "tp"), None),
        P(),
        P("fs", "tp"),
        P("fs", "tp"),
        P("tp", "fs"),
        P(),
        P("fs", "tp"),
        P("fs", "tp"),
        P("tp", "fs"),
    )
    out_specs = P(("grp", "fs", "tp"), None)
    return jax.shard_map(local, mesh=mesh, in_specs=in_specs, out_specs=out_specs, check_vma=False)
```

profile of v0, /device:TPU:0, one launch (start us, length us, event | category | flops | bytes accessed | tf_op | source)
XLA Modules:
  0.0 435.7 jit_solution(18074914909830998530)
XLA Ops:
  6.5 0.0 all-gather.9.cloned.1.call-start
  6.5 0.7 convert_element_type.43
  7.2 1.2 fusion
  8.5 2.0 fusion.2
  10.5 0.0 all-gather.9.cloned.1.call-update
  10.5 0.0 all-gather.11.cloned.1.call-start
  10.6 0.7 all-gather.11.cloned.1.call-update
  11.3 0.0 all-gather.13.cloned.1.call-start
  11.3 0.7 all-gather.13.cloned.1.call-update
  12.0 0.0 all-gather.15.cloned.1.call-start
  12.0 0.5 all-gather.15.cloned.1.call-update
  12.6 0.0 reduce-scatter.3.cloned.1.call-start
  12.6 46.4 %all-gather.9.cloned.1.call-done = bf16[512,2048]{1,0:T(8,128)(2,1)} async-done(((bf16[128,2048]{1,0:T(8,128)(2,1)}), bf16[512,2048]{1,0:T(8,128)(2,1)}) %all-gather.9.cloned.1.call-update) | async-done | bytes 2097168 | tf_op jit(solution)/shard_map/all_gather | solution.py:14
  59.1 0.0 copy-start.3
  59.1 34.9 %all-gather.11.cloned.1.call-done = bf16[2048,1024]{1,0:T(8,128)(2,1)} async-done(((bf16[512,1024]{1,0:T(8,128)(2,1)}), bf16[2048,1024]{1,0:T(8,128)(2,1)}) %all-gather.11.cloned.1.call-update) | async-done | bytes 4194320 | tf_op jit(solution)/shard_map/all_gather | solution.py:40
  93.9 6.5 %fusion.10 = f32[512,1024]{1,0:T(8,128)} fusion(bf16[512,2048]{1,0:T(8,128)(2,1)} %all-gather.9.cloned.1.call-done, bf16[2048,1024]{1,0:T(8,128)(2,1)} %all-gather.11.cloned.1.call-done), kind=kOutput, calls=%fused_computation.22 | convolution fusion | flops 2147483648 | bytes 8388608 | tf_op jit(solution)/shard_map/dot_general | solution.py:15
  100.4 29.6 %all-gather.13.cloned.1.call-done = bf16[2048,1024]{1,0:T(8,128)(2,1)} async-done(((bf16[512,1024]{1,0:T(8,128)(2,1)}), bf16[2048,1024]{1,0:T(8,128)(2,1)}) %all-gather.13.cloned.1.call-update) | async-done | bytes 4194320 | tf_op jit(solution)/shard_map/all_gather | solution.py:41
  130.0 35.9 %all-gather.15.cloned.1.call-done = bf16[1024,2048]{1,0:T(8,128)(2,1)} async-done(((bf16[1024,512]{1,0:T(8,128)(2,1)}), bf16[1024,2048]{1,0:T(8,128)(2,1)}) %all-gather.15.cloned.1.call-update) | async-done | bytes 4194320 | tf_op jit(solution)/shard_map/all_gather | solution.py:42
  165.9 0.0 copy-done.3
  165.9 10.0 %convolution_convert_fusion.1 = bf16[512,2048]{1,0:T(8,128)(2,1)} fusion(bf16[1024,2048]{1,0:T(8,128)(2,1)} %all-gather.15.cloned.1.call-done, f32[512,1024]{1,0:T(8,128)} %fusion.10, bf16[512,2048]{1,0:T(8,128)(2,1)S(1)} %copy-done.3, bf16[2048,1024]{1,0:T(8,128)(2,1)} %all-gather.13.cloned.1.call-done), kind=kOutput, calls=%fused_computation.1 | convolution fusion | flops 4299161600 | bytes 14680064 | tf_op jit(solution)/shard_map/dot_general | solution.py:20
  175.9 0.0 copy-start.2
  175.9 0.0 copy-start
  175.9 0.0 reduce-scatter.3.cloned.1.call-update
  175.9 0.0 all-gather.19.cloned.1.call-start
  175.9 0.5 all-gather.19.cloned.1.call-update
  176.5 0.0 all-gather.17.cloned.1.call-start
  176.5 0.0 copy-done.2
  176.6 43.1 %reduce-scatter.3.cloned.1.call-done = bf16[128,2048]{1,0:T(8,128)(2,1)} async-done(((bf16[512,2048]{1,0:T(8,128)(2,1)}), bf16[128,2048]{1,0:T(8,128)(2,1)}) %reduce-scatter.3.cloned.1.call-update) | async-done | bytes 524304 | tf_op jit(solution)/shard_map/reduce_scatter | solution.py:19
  219.7 0.0 copy-done
  219.7 1.3 fusion.4
  221.0 2.1 fusion.6
  223.1 0.0 all-gather.17.cloned.1.call-update
  223.1 0.0 all-gather.21.cloned.1.call-start
  223.2 0.7 all-gather.21.cloned.1.call-update
  223.9 0.0 all-gather.23.cloned.1.call-start
  223.9 0.7 all-gather.23.cloned.1.call-update
  224.6 0.2 reduce-scatter.5.cloned.1.call-start
  224.8 30.0 %all-gather.19.cloned.1.call-done = bf16[2048,1024]{1,0:T(8,128)(2,1)} async-done(((bf16[512,1024]{1,0:T(8,128)(2,1)}), bf16[2048,1024]{1,0:T(8,128)(2,1)}) %all-gather.19.cloned.1.call-update) | async-done | bytes 4194320 | tf_op jit(solution)/shard_map/all_gather | solution.py:43
  254.8 47.3 %all-gather.17.cloned.1.call-done = bf16[512,2048]{1,0:T(8,128)(2,1)} async-done(((bf16[128,2048]{1,0:T(8,128)(2,1)}), bf16[512,2048]{1,0:T(8,128)(2,1)}) %all-gather.17.cloned.1.call-update) | async-done | bytes 2097168 | tf_op jit(solution)/shard_map/all_gather | solution.py:14
  302.1 6.6 %fusion.11 = f32[512,1024]{1,0:T(8,128)} fusion(bf16[512,2048]{1,0:T(8,128)(2,1)} %all-gather.17.cloned.1.call-done, bf16[2048,1024]{1,0:T(8,128)(2,1)} %all-gather.19.cloned.1.call-done), kind=kOutput, calls=%fused_computation.23 | convolution fusion | flops 2147483648 | bytes 8388608 | tf_op jit(solution)/shard_map/dot_general | solution.py:15
  308.7 28.2 %all-gather.21.cloned.1.call-done = bf16[2048,1024]{1,0:T(8,128)(2,1)} async-done(((bf16[512,1024]{1,0:T(8,128)(2,1)}), bf16[2048,1024]{1,0:T(8,128)(2,1)}) %all-gather.21.cloned.1.call-update) | async-done | bytes 4194320 | tf_op jit(solution)/shard_map/all_gather | solution.py:44
  336.9 36.1 %all-gather.23.cloned.1.call-done = bf16[1024,2048]{1,0:T(8,128)(2,1)} async-done(((bf16[1024,512]{1,0:T(8,128)(2,1)}), bf16[1024,2048]{1,0:T(8,128)(2,1)}) %all-gather.23.cloned.1.call-update) | async-done | bytes 4194320 | tf_op jit(solution)/shard_map/all_gather | solution.py:45
  373.0 0.0 copy-done.4
  373.0 9.9 %convolution_convert_fusion = bf16[512,2048]{1,0:T(8,128)(2,1)} fusion(bf16[1024,2048]{1,0:T(8,128)(2,1)} %all-gather.23.cloned.1.call-done, f32[512,1024]{1,0:T(8,128)} %fusion.11, bf16[512,2048]{1,0:T(8,128)(2,1)S(1)} %copy-done.4, bf16[2048,1024]{1,0:T(8,128)(2,1)} %all-gather.21.cloned.1.call-done), kind=kOutput, calls=%fused_computation | convolution fusion | flops 4299161600 | bytes 14680064 | tf_op jit(solution)/shard_map/dot_general | solution.py:20
  382.9 0.0 reduce-scatter.5.cloned.1.call-update
  382.9 43.8 %reduce-scatter.5.cloned.1.call-done = bf16[128,2048]{1,0:T(8,128)(2,1)} async-done(((bf16[512,2048]{1,0:T(8,128)(2,1)}), bf16[128,2048]{1,0:T(8,128)(2,1)}) %reduce-scatter.5.cloned.1.call-update) | async-done | bytes 524304 | tf_op jit(solution)/shard_map/reduce_scatter | solution.py:19
  426.7 0.0 copy-done.1
  426.7 2.1 fusion.7
  (5 shorter events, 0.0 us)
Async XLA Ops:
  6.5 52.5 %all-gather.9.cloned.1.call-start = ((), (), s32[]{:S(2)}) async-start(), calls=%async_computation.2 | async-start | bytes 2621440 | tf_op jit(solution)/shard_map/all_gather | solution.py:14
  10.5 83.4 %all-gather.11.cloned.1.call-start = ((), (), s32[]{:S(2)}) async-start(), calls=%async_computation.3 | async-start | bytes 5242880 | tf_op jit(solution)/shard_map/all_gather | solution.py:40
  11.3 118.7 %all-gather.13.cloned.1.call-start = ((), (), s32[]{:S(2)}) async-start(), calls=%async_computation.4 | async-start | bytes 5242880 | tf_op jit(solution)/shard_map/all_gather | solution.py:41
  12.0 153.9 %all-gather.15.cloned.1.call-start = ((), (), s32[]{:S(2)}) async-start(), calls=%async_computation.5 | async-start | bytes 5242880 | tf_op jit(solution)/shard_map/all_gather | solution.py:42
  12.6 207.1 %reduce-scatter.3.cloned.1.call-start = ((), (), s32[]{:S(2)}) async-start(), calls=%async_computation.6 | async-start | bytes 2621440 | tf_op jit(solution)/shard_map/reduce_scatter | solution.py:19
  59.1 106.8 %copy-start.3 = (bf16[512,2048]{1,0:T(8,128)(2,1)S(1)}, bf16[512,2048]{1,0:T(8,128)(2,1)}, u32[]{:S(2)}) copy-start(bf16[512,2048]{1,0:T(8,128)(2,1)} %all-gather.9.cloned.1.call-done) | copy-start | bytes 6291460
  175.9 0.7 copy-start.2
  175.9 43.8 %copy-start = (bf16[128,2048]{1,0:T(8,128)(2,1)S(1)}, bf16[128,2048]{1,0:T(8,128)(2,1)}, u32[]{:S(2)}) copy-start(bf16[128,2048]{1,0:T(8,128)(2,1)} %param.9) | copy-start | bytes 1572868
  175.9 78.9 %all-gather.19.cloned.1.call-start = ((), (), s32[]{:S(2)}) async-start(), calls=%async_computation.8 | async-start | bytes 5242880 | tf_op jit(solution)/shard_map/all_gather | solution.py:43
  176.5 125.6 %all-gather.17.cloned.1.call-start = ((), (), s32[]{:S(2)}) async-start(), calls=%async_computation.7 | async-start | bytes 2621440 | tf_op jit(solution)/shard_map/all_gather | solution.py:14
  223.1 113.8 %all-gather.21.cloned.1.call-start = ((), (), s32[]{:S(2)}) async-start(), calls=%async_computation.9 | async-start | bytes 5242880 | tf_op jit(solution)/shard_map/all_gather | solution.py:44
  223.9 149.1 %all-gather.23.cloned.1.call-start = ((), (), s32[]{:S(2)}) async-start(), calls=%async_computation.10 | async-start | bytes 5242880 | tf_op jit(solution)/shard_map/all_gather | solution.py:45
  224.6 202.1 %reduce-scatter.5.cloned.1.call-start = ((), (), s32[]{:S(2)}) async-start(), calls=%async_computation.11 | async-start | bytes 2621440 | tf_op jit(solution)/shard_map/reduce_scatter | solution.py:19
  302.1 70.9 %copy-start.4 = (bf16[512,2048]{1,0:T(8,128)(2,1)S(1)}, bf16[512,2048]{1,0:T(8,128)(2,1)}, u32[]{:S(2)}) copy-start(bf16[512,2048]{1,0:T(8,128)(2,1)} %all-gather.17.cloned.1.call-done) | copy-start | bytes 6291460
  382.9 43.8 %copy-start.1 = (bf16[128,2048]{1,0:T(8,128)(2,1)S(1)}, bf16[128,2048]{1,0:T(8,128)(2,1)}, u32[]{:S(2)}) copy-start(bf16[128,2048]{1,0:T(8,128)(2,1)} %reduce-scatter.3.cloned.1.call-done) | copy-start | bytes 1572868
Sparse Core Ops, SparseCore 0:
  10.6 48.3 all-gather.8
  60.6 33.2 all-gather.10
  95.5 34.4 all-gather.12
  131.4 34.4 all-gather.14
  176.0 43.6 reduce-scatter.2
  221.1 33.6 all-gather.18
  256.4 45.6 all-gather.16
  303.6 33.2 all-gather.20
  338.5 34.4 all-gather.22
  383.0 43.6 reduce-scatter.4
where the time goes:
time: 436 us
  waiting for transfers between devices  379 us (87%)
  matrix products  33 us (8%)
  between operations  13.5 us (3%)
  other arithmetic  9.46 us (2%)
    all_gather x2, waiting for transfers between devices, half_branch(): tokens = lax.all_gather(normed, 'tp', axis=0, tiled=True)  93.7 us
    reduce_scatter x2, waiting for transfers between devices, half_branch(): lax.psum_scatter(jnp.dot(hidden, down_full, preferred_element_type=jnp.fl...  86.9 us
    all_gather x1, waiting for transfers between devices, local(): lax.all_gather(down_second, 'fs', axis=1, tiled=True)  36.1 us
    all_gather x1, waiting for transfers between devices, local(): lax.all_gather(down_first, 'fs', axis=1, tiled=True)  35.9 us
    all_gather x1, waiting for transfers between devices, local(): lax.all_gather(gate_first, 'fs', axis=0, tiled=True)  34.9 us
    all_gather x1, waiting for transfers between devices, local(): lax.all_gather(gate_second, 'fs', axis=0, tiled=True)  30 us
    all_gather x1, waiting for transfers between devices, local(): lax.all_gather(up_first, 'fs', axis=0, tiled=True)  29.6 us
    all_gather x1, waiting for transfers between devices, local(): lax.all_gather(up_second, 'fs', axis=0, tiled=True)  28.2 us
  transfers between devices with their start and end apart: 10, of which 10 were waited for; matrix products, arithmetic and copies ran while one was open for 4% of the time, Pallas kernels for 0%

commit v1 on v0

--- a/solution.py
+++ b/solution.py
@@ -1,7 +1,28 @@
+import functools
 import jax
 import jax.numpy as jnp
 from jax import lax
 from jax.sharding import PartitionSpec as P
+
+
+def keep_up_stacks_all_on_mesh(in_array, lane_axis, in_dim):
+    n_chips = lax.psum(1, lane_axis)
+    found = [in_array]
+    for dd in [*range(n_chips - 1)]:
+        found.append(
+            lax.ppermute(
+                found[-1],
+                axis_name=lane_axis,
+                perm=[(j0, (j0 + 1) % n_chips) for j0 in range(n_chips)],
+            )
+        )
+    p_next = jnp.concatenate(found[::-1], axis=in_dim)
+    return jnp.roll(
+        p_next, shift=(lax.axis_index(lane_axis) + 1) * in_array.shape[in_dim], axis=in_dim
+    )
+
+
+strings_put = functools.partial(keep_up_stacks_all_on_mesh, lane_axis="tp", in_dim=0)
 
 
 def half_branch(stream, gain, gathered):
@@ -11,7 +32,7 @@
         * lax.rsqrt(jnp.mean(stream_f * stream_f, axis=-1, keepdims=True) + 1e-06)
         * gain.astype(jnp.float32)
     ).astype(jnp.bfloat16)
-    tokens = lax.all_gather(normed, "tp", axis=0, tiled=True)
+    tokens = strings_put(normed)
     gate_act = jnp.dot(tokens, gathered[0], preferred_element_type=jnp.float32)
     up_act = jnp.dot(tokens, gathered[1], preferred_element_type=jnp.float32)
     down_full = gathered[2]

time: 436 us -> 342 us (0.78)
  waiting for transfers between devices: 379 us -> 267 us
  other arithmetic: 9.46 us -> 24.2 us
    all_gather x2 -> x0, waiting for transfers between devices: 93.7 us -> none  [half_branch(): tokens = lax.all_gather(normed, 'tp', axis=0, tiled=True)]
    ppermute x0 -> x6, waiting for transfers between devices: none -> 84.1 us  [keep_up_stacks_all_on_mesh(): lax.ppermute(found[-1], axis_name=lane_axis, perm=[(j0, (j0 + 1) % n_chip...]
    all_gather x1, waiting for transfers between devices: 34.9 us -> 0.02 us  [local(): lax.all_gather(gate_first, 'fs', axis=0, tiled=True)]
    all_gather x1, waiting for transfers between devices: 30 us -> 0.02 us  [local(): lax.all_gather(gate_second, 'fs', axis=0, tiled=True)]
    all_gather x1, waiting for transfers between devices: 35.9 us -> 10.4 us  [local(): lax.all_gather(down_first, 'fs', axis=1, tiled=True)]
    all_gather x1, waiting for transfers between devices: 28.2 us -> 11.4 us  [local(): lax.all_gather(up_second, 'fs', axis=0, tiled=True)]
    concatenate x0 -> x2, other arithmetic: none -> 16.3 us  [keep_up_stacks_all_on_mesh(): jnp.roll(p_next, shift=(lax.axis_index(lane_axis) + 1) * in_array.shape[i...]
    all_gather x1, waiting for transfers between devices: 29.6 us -> 36.1 us  [local(): lax.all_gather(up_first, 'fs', axis=0, tiled=True)]
  transfers between devices with their start and end apart: 10 -> 14, of which waited for: 10 -> 12; matrix products, arithmetic and copies ran while one was open for 4% -> 10% of each run, Pallas kernels for 0% -> 0%
where the time goes in v1:
time: 342 us
  waiting for transfers between devices  267 us (78%)
  matrix products  31.6 us (9%)
  other arithmetic  24.2 us (7%)
  between operations  13.6 us (4%)
  starting transfers between devices  4.11 us (1%)
    reduce_scatter x2, waiting for transfers between devices, half_branch(): lax.psum_scatter(jnp.dot(hidden, down_full, preferred_element_type=jnp.fl...  85.5 us
    ppermute x6, waiting for transfers between devices, keep_up_stacks_all_on_mesh(): lax.ppermute(found[-1], axis_name=lane_axis, perm=[(j0, (j0 + 1) % n_chip...  84.1 us
    all_gather x1, waiting for transfers between devices, local(): lax.all_gather(up_first, 'fs', axis=0, tiled=True)  36.1 us
    all_gather x1, waiting for transfers between devices, local(): lax.all_gather(down_second, 'fs', axis=1, tiled=True)  36 us
    dot_general x2, matrix products, half_branch(): jnp.dot(hidden, down_full, preferred_element_type=jnp.float32)  19.9 us
    concatenate x2, other arithmetic, keep_up_stacks_all_on_mesh(): jnp.roll(p_next, shift=(lax.axis_index(lane_axis) + 1) * in_array.shape[i...  16.3 us
    dot_general x2, matrix products, half_branch(): gate_act = jnp.dot(tokens, gathered[0], preferred_element_type=jnp.float32)  11.7 us
    all_gather x1, waiting for transfers between devices, local(): lax.all_gather(up_second, 'fs', axis=0, tiled=True)  11.4 us
  transfers between devices with their start and end apart: 14, of which 12 were waited for; matrix products, arithmetic and copies ran while one was open for 10% of the time, Pallas kernels for 0%

profile of v1, /device:TPU:0, one launch (start us, length us, event | category | flops | bytes accessed | tf_op | source)
XLA Modules:
  0.0 341.7 jit_solution(17754355353690746145)
XLA Ops:
  6.5 0.7 all-gather.7.cloned.1.call-update
  7.3 0.0 all-gather.11.cloned.1.call-start
  7.3 0.7 all-gather.11.cloned.1.call-update
  8.0 0.0 all-gather.9.cloned.1.call-start
  8.1 0.7 all-gather.9.cloned.1.call-update
  8.7 0.0 reduce-scatter.3.cloned.1.call-start
  8.8 0.7 convert_element_type.43
  9.5 1.2 fusion.14
  10.7 1.2 fusion.16
  12.0 3.1 collective-permute-start
  15.1 13.9 %collective-permute-done = bf16[128,2048]{1,0:T(8,128)(2,1)S(1)} collective-permute-done((bf16[128,2048]{1,0:T(8,128)(2,1)S(1)}, bf16[128,2048]{1,0:T(8,128)(2,1)S(1)}, u32[]{:S(2)}, u32[]{:S(2)}) %collective-permute-start) | collective-permute-done | bytes 524320 | tf_op jit(solution)/shard_map/ppermute | solution.py:13
  29.0 0.0 collective-permute-start.1
  29.0 14.9 %collective-permute-done.1 = bf16[128,2048]{1,0:T(8,128)(2,1)S(1)} collective-permute-done((bf16[128,2048]{1,0:T(8,128)(2,1)S(1)}, bf16[128,2048]{1,0:T(8,128)(2,1)S(1)}, u32[]{:S(2)}, u32[]{:S(2)}) %collective-permute-start.1) | collective-permute-done | bytes 524320 | tf_op jit(solution)/shard_map/ppermute | solution.py:13
  43.9 0.0 collective-permute-start.2
  43.9 0.8 copy-done.2
  44.7 13.3 %collective-permute-done.2 = bf16[128,2048]{1,0:T(8,128)(2,1)} collective-permute-done((bf16[128,2048]{1,0:T(8,128)(2,1)S(1)}, bf16[128,2048]{1,0:T(8,128)(2,1)}, u32[]{:S(2)}, u32[]{:S(2)}) %collective-permute-start.2) | collective-permute-done | bytes 524320 | tf_op jit(solution)/shard_map/ppermute | solution.py:13
  58.0 7.9 %fusion.10 = bf16[512,2048]{1,0:T(8,128)(2,1)S(1)} fusion(s32[]{:T(128)S(6)} %select_n.13, bf16[128,2048]{1,0:T(8,128)(2,1)} %collective-permute-done.2, bf16[128,2048]{1,0:T(8,128)(2,1)} %copy-done.2, bf16[128,2048]{1,0:T(8,128)(2,1)S(1)} %collective-permute-done, bf16[128,2048]{1,0:T(8,128)(2,1)S(1)} %fusion.16), kind=kLoop, calls=%fused_computation.28 | loop fusion | flops 16777216 | bytes 4194308 | tf_op jit(solution)/shard_map/jit(_roll_dynamic)/concatenate | solution.py:20
  65.9 0.0 all-gather.7.cloned.1.call-done
  66.0 5.8 %fusion.24 = f32[512,1024]{1,0:T(8,128)} fusion(bf16[512,2048]{1,0:T(8,128)(2,1)S(1)} %fusion.10, bf16[2048,1024]{1,0:T(8,128)(2,1)} %all-gather.7.cloned.1.call-done), kind=kOutput, calls=%fused_computation.52 | convolution fusion | flops 2147483648 | bytes 8388608 | tf_op jit(solution)/shard_map/dot_general | solution.py:36
  71.8 10.4 %all-gather.11.cloned.1.call-done = bf16[1024,2048]{1,0:T(8,128)(2,1)} async-done(((bf16[1024,512]{1,0:T(8,128)(2,1)}), bf16[1024,2048]{1,0:T(8,128)(2,1)}) %all-gather.11.cloned.1.call-update) | async-done | bytes 4194320 | tf_op jit(solution)/shard_map/all_gather | solution.py:63
  82.2 36.1 %all-gather.9.cloned.1.call-done = bf16[2048,1024]{1,0:T(8,128)(2,1)} async-done(((bf16[512,1024]{1,0:T(8,128)(2,1)}), bf16[2048,1024]{1,0:T(8,128)(2,1)}) %all-gather.9.cloned.1.call-update) | async-done | bytes 4194320 | tf_op jit(solution)/shard_map/all_gather | solution.py:62
  118.2 9.9 %convolution_convert_fusion.1 = bf16[512,2048]{1,0:T(8,128)(2,1)} fusion(bf16[1024,2048]{1,0:T(8,128)(2,1)} %all-gather.11.cloned.1.call-done, f32[512,1024]{1,0:T(8,128)} %fusion.24, bf16[512,2048]{1,0:T(8,128)(2,1)S(1)} %fusion.10, bf16[2048,1024]{1,0:T(8,128)(2,1)} %all-gather.9.cloned.1.call-done), kind=kOutput, calls=%fused_computation.17 | convolution fusion | flops 4299161600 | bytes 14680064 | tf_op jit(solution)/shard_map/dot_general | solution.py:41
  128.2 0.0 reduce-scatter.3.cloned.1.call-update
  128.2 0.0 all-gather.13.cloned.1.call-start
  128.2 0.5 all-gather.13.cloned.1.call-update
  128.8 0.0 all-gather.15.cloned.1.call-start
  128.8 0.5 all-gather.15.cloned.1.call-update
  129.3 0.0 all-gather.17.cloned.1.call-start
  129.4 0.7 all-gather.17.cloned.1.call-update
  130.1 0.0 reduce-scatter.5.cloned.1.call-start
  130.2 41.8 %reduce-scatter.3.cloned.1.call-done = bf16[128,2048]{1,0:T(8,128)(2,1)} async-done(((bf16[512,2048]{1,0:T(8,128)(2,1)}), bf16[128,2048]{1,0:T(8,128)(2,1)}) %reduce-scatter.3.cloned.1.call-update) | async-done | bytes 524304 | tf_op jit(solution)/shard_map/reduce_scatter | solution.py:40
  171.9 1.3 fusion.18
  173.3 1.3 fusion.20
  174.6 0.7 collective-permute-start.3
  175.3 14.4 %collective-permute-done.3 = bf16[128,2048]{1,0:T(8,128)(2,1)S(1)} collective-permute-done((bf16[128,2048]{1,0:T(8,128)(2,1)S(1)}, bf16[128,2048]{1,0:T(8,128)(2,1)S(1)}, u32[]{:S(2)}, u32[]{:S(2)}) %collective-permute-start.3) | collective-permute-done | bytes 524320 | tf_op jit(solution)/shard_map/ppermute | solution.py:13
  189.7 0.0 collective-permute-start.4
  189.7 14.2 %collective-permute-done.4 = bf16[128,2048]{1,0:T(8,128)(2,1)S(1)} collective-permute-done((bf16[128,2048]{1,0:T(8,128)(2,1)S(1)}, bf16[128,2048]{1,0:T(8,128)(2,1)S(1)}, u32[]{:S(2)}, u32[]{:S(2)}) %collective-permute-start.4) | collective-permute-done | bytes 524320 | tf_op jit(solution)/shard_map/ppermute | solution.py:13
  203.9 0.0 collective-permute-start.5
  203.9 13.4 %collective-permute-done.5 = bf16[128,2048]{1,0:T(8,128)(2,1)S(1)} collective-permute-done((bf16[128,2048]{1,0:T(8,128)(2,1)S(1)}, bf16[128,2048]{1,0:T(8,128)(2,1)S(1)}, u32[]{:S(2)}, u32[]{:S(2)}) %collective-permute-start.5) | collective-permute-done | bytes 524320 | tf_op jit(solution)/shard_map/ppermute | solution.py:13
  217.3 8.4 %fusion.3 = bf16[512,2048]{1,0:T(8,128)(2,1)S(1)} fusion(s32[]{:T(128)S(6)} %select_n.13, bf16[128,2048]{1,0:T(8,128)(2,1)S(1)} %collective-permute-done.5, bf16[128,2048]{1,0:T(8,128)(2,1)S(1)} %collective-permute-done.4, bf16[128,2048]{1,0:T(8,128)(2,1)S(1)} %collective-permute-done.3, bf16[128,2048]{1,0:T(8,128)(2,1)S(1)} %fusion.20), kind=kLoop, calls=%fused_computation.21 | loop fusion | flops 16777216 | bytes 4194308 | tf_op jit(solution)/shard_map/jit(_roll_dynamic)/concatenate | solution.py:20
  225.7 0.0 all-gather.13.cloned.1.call-done
  225.7 5.8 %fusion.25 = f32[512,1024]{1,0:T(8,128)} fusion(bf16[512,2048]{1,0:T(8,128)(2,1)S(1)} %fusion.3, bf16[2048,1024]{1,0:T(8,128)(2,1)} %all-gather.13.cloned.1.call-done), kind=kOutput, calls=%fused_computation.53 | convolution fusion | flops 2147483648 | bytes 8388608 | tf_op jit(solution)/shard_map/dot_general | solution.py:36
  231.5 11.4 %all-gather.15.cloned.1.call-done = bf16[2048,1024]{1,0:T(8,128)(2,1)} async-done(((bf16[512,1024]{1,0:T(8,128)(2,1)}), bf16[2048,1024]{1,0:T(8,128)(2,1)}) %all-gather.15.cloned.1.call-update) | async-done | bytes 4194320 | tf_op jit(solution)/shard_map/all_gather | solution.py:65
  242.9 36.0 %all-gather.17.cloned.1.call-done = bf16[1024,2048]{1,0:T(8,128)(2,1)} async-done(((bf16[1024,512]{1,0:T(8,128)(2,1)}), bf16[1024,2048]{1,0:T(8,128)(2,1)}) %all-gather.17.cloned.1.call-update) | async-done | bytes 4194320 | tf_op jit(solution)/shard_map/all_gather | solution.py:66
  279.0 10.0 %convolution_convert_fusion = bf16[512,2048]{1,0:T(8,128)(2,1)} fusion(bf16[1024,2048]{1,0:T(8,128)(2,1)} %all-gather.17.cloned.1.call-done, f32[512,1024]{1,0:T(8,128)} %fusion.25, bf16[512,2048]{1,0:T(8,128)(2,1)S(1)} %fusion.3, bf16[2048,1024]{1,0:T(8,128)(2,1)} %all-gather.15.cloned.1.call-done), kind=kOutput, calls=%fused_computation.16 | convolution fusion | flops 4299161600 | bytes 14680064 | tf_op jit(solution)/shard_map/dot_general | solution.py:41
  289.0 0.0 reduce-scatter.5.cloned.1.call-update
  289.0 43.8 %reduce-scatter.5.cloned.1.call-done = bf16[128,2048]{1,0:T(8,128)(2,1)} async-done(((bf16[512,2048]{1,0:T(8,128)(2,1)}), bf16[128,2048]{1,0:T(8,128)(2,1)}) %reduce-scatter.5.cloned.1.call-update) | async-done | bytes 524304 | tf_op jit(solution)/shard_map/reduce_scatter | solution.py:40
  332.8 2.1 fusion.21
  (11 shorter events, 0.0 us)
Async XLA Ops:
  6.5 59.4 %all-gather.7.cloned.1.call-start = ((), (), s32[]{:S(2)}) async-start(), calls=%async_computation.2 | async-start | bytes 5242880 | tf_op jit(solution)/shard_map/all_gather | solution.py:61
  7.3 74.9 %all-gather.11.cloned.1.call-start = ((), (), s32[]{:S(2)}) async-start(), calls=%async_computation.4 | async-start | bytes 5242880 | tf_op jit(solution)/shard_map/all_gather | solution.py:63
  8.0 110.2 %all-gather.9.cloned.1.call-start = ((), (), s32[]{:S(2)}) async-start(), calls=%async_computation.3 | async-start | bytes 5242880 | tf_op jit(solution)/shard_map/all_gather | solution.py:62
  8.7 163.2 %reduce-scatter.3.cloned.1.call-start = ((), (), s32[]{:S(2)}) async-start(), calls=%async_computation.5 | async-start | bytes 2621440 | tf_op jit(solution)/shard_map/reduce_scatter | solution.py:40
  12.0 17.1 %collective-permute-start = (bf16[128,2048]{1,0:T(8,128)(2,1)S(1)}, bf16[128,2048]{1,0:T(8,128)(2,1)S(1)}, u32[]{:S(2)}, u32[]{:S(2)}) collective-permute-start(bf16[128,2048]{1,0:T(8,128)(2,1)S(1)} %fusion.16), channel_id=1, source_target_pairs={{0,1},{1,2},{2,3},{3,0},{4,5},{5,6},{6,7},{7,4},{8,9},{9,10},{10,1... | collective-permute-start | bytes 1572872 | tf_op jit(solution)/shard_map/ppermute | solution.py:13
  29.0 14.9 %collective-permute-start.1 = (bf16[128,2048]{1,0:T(8,128)(2,1)S(1)}, bf16[128,2048]{1,0:T(8,128)(2,1)S(1)}, u32[]{:S(2)}, u32[]{:S(2)}) collective-permute-start(bf16[128,2048]{1,0:T(8,128)(2,1)S(1)} %collective-permute-done), channel_id=1, source_target_pairs={{0,1},{1,2},{2,3},{3,0},{4,5},{5,6},{6,7},{7,4},{8,9},{9,10},{10,1... | collective-permute-start | bytes 1572872 | tf_op jit(solution)/shard_map/ppermute | solution.py:13
  43.9 0.8 copy-start.2
  43.9 14.1 %collective-permute-start.2 = (bf16[128,2048]{1,0:T(8,128)(2,1)S(1)}, bf16[128,2048]{1,0:T(8,128)(2,1)}, u32[]{:S(2)}, u32[]{:S(2)}) collective-permute-start(bf16[128,2048]{1,0:T(8,128)(2,1)S(1)} %collective-permute-done.1), channel_id=1, source_target_pairs={{0,1},{1,2},{2,3},{3,0},{4,5},{5,6},{6,7},{7,4},{8,9},{9,10},{10,1... | collective-permute-start | bytes 1572872 | tf_op jit(solution)/shard_map/ppermute | solution.py:13
  128.1 2.0 copy-start.3
  128.2 43.8 %copy-start = (bf16[128,2048]{1,0:T(8,128)(2,1)S(1)}, bf16[128,2048]{1,0:T(8,128)(2,1)}, u32[]{:S(2)}) copy-start(bf16[128,2048]{1,0:T(8,128)(2,1)} %param.11) | copy-start | bytes 1572868
  128.2 97.5 %all-gather.13.cloned.1.call-start = ((), (), s32[]{:S(2)}) async-start(), calls=%async_computation.6 | async-start | bytes 5242880 | tf_op jit(solution)/shard_map/all_gather | solution.py:64
  128.8 114.2 %all-gather.15.cloned.1.call-start = ((), (), s32[]{:S(2)}) async-start(), calls=%async_computation.7 | async-start | bytes 5242880 | tf_op jit(solution)/shard_map/all_gather | solution.py:65
  129.3 149.7 %all-gather.17.cloned.1.call-start = ((), (), s32[]{:S(2)}) async-start(), calls=%async_computation.8 | async-start | bytes 5242880 | tf_op jit(solution)/shard_map/all_gather | solution.py:66
  130.1 202.7 %reduce-scatter.5.cloned.1.call-start = ((), (), s32[]{:S(2)}) async-start(), calls=%async_computation.9 | async-start | bytes 2621440 | tf_op jit(solution)/shard_map/reduce_scatter | solution.py:40
  174.6 15.1 %collective-permute-start.3 = (bf16[128,2048]{1,0:T(8,128)(2,1)S(1)}, bf16[128,2048]{1,0:T(8,128)(2,1)S(1)}, u32[]{:S(2)}, u32[]{:S(2)}) collective-permute-start(bf16[128,2048]{1,0:T(8,128)(2,1)S(1)} %fusion.20), channel_id=1, source_target_pairs={{0,1},{1,2},{2,3},{3,0},{4,5},{5,6},{6,7},{7,4},{8,9},{9,10},{10,1... | collective-permute-start | bytes 1572872 | tf_op jit(solution)/shard_map/ppermute | solution.py:13
  189.7 14.2 %collective-permute-start.4 = (bf16[128,2048]{1,0:T(8,128)(2,1)S(1)}, bf16[128,2048]{1,0:T(8,128)(2,1)S(1)}, u32[]{:S(2)}, u32[]{:S(2)}) collective-permute-start(bf16[128,2048]{1,0:T(8,128)(2,1)S(1)} %collective-permute-done.3), channel_id=1, source_target_pairs={{0,1},{1,2},{2,3},{3,0},{4,5},{5,6},{6,7},{7,4},{8,9},{9,10},{10,1... | collective-permute-start | bytes 1572872 | tf_op jit(solution)/shard_map/ppermute | solution.py:13
  203.9 13.4 %collective-permute-start.5 = (bf16[128,2048]{1,0:T(8,128)(2,1)S(1)}, bf16[128,2048]{1,0:T(8,128)(2,1)S(1)}, u32[]{:S(2)}, u32[]{:S(2)}) collective-permute-start(bf16[128,2048]{1,0:T(8,128)(2,1)S(1)} %collective-permute-done.4), channel_id=1, source_target_pairs={{0,1},{1,2},{2,3},{3,0},{4,5},{5,6},{6,7},{7,4},{8,9},{9,10},{10,1... | collective-permute-start | bytes 1572872 | tf_op jit(solution)/shard_map/ppermute | solution.py:13
  231.5 101.3 %copy-start.1 = (bf16[128,2048]{1,0:T(8,128)(2,1)S(1)}, bf16[128,2048]{1,0:T(8,128)(2,1)}, u32[]{:S(2)}) copy-start(bf16[128,2048]{1,0:T(8,128)(2,1)} %reduce-scatter.3.cloned.1.call-done) | copy-start | bytes 1572868
Sparse Core Ops, SparseCore 0:
  8.9 37.1 all-gather.6
  47.7 34.4 all-gather.10
  83.7 34.4 all-gather.8
  128.3 43.5 reduce-scatter.2
  173.3 33.6 all-gather.12
  208.5 34.4 all-gather.14
  244.5 34.4 all-gather.16
  289.1 43.5 reduce-scatter.4
